TPU v7x, 32 devices: a whole 2x2x4 slice. The times are simulated.
32 devices in a mesh: sp: 8 (over z, x), tp: 4 (over y, core).
Axes of the slice: x: 2, y: 2, z: 4, core: 2. Of those that a mesh axis runs over, the one named last changes fastest.
Arguments:
- rows_in: bfloat16 [1024, 2048], P(('sp', 'tp')), may hold values from -8 to 8
- in_gain: float32 [2048], replicated, may hold values from 0.1 to 1.9
- query_down: bfloat16 [2048, 256], replicated, may hold values from -0.125 to 0.125
- query_gain: float32 [256], replicated, may hold values from 0.1 to 1.9
- kv_down: bfloat16 [2048, 128], replicated, may hold values from -0.125 to 0.125
- kv_gain: float32 [128], replicated, may hold values from 0.1 to 1.9
- rope_down: bfloat16 [2048, 64], replicated, may hold values from -0.125 to 0.125
- query_nope_up: bfloat16 [256, 512], P(None, 'tp'), may hold values from -0.375 to 0.375
- query_rope_up: bfloat16 [256, 256], P(None, 'tp'), may hold values from -0.375 to 0.375
- key_up: bfloat16 [128, 512], P(None, 'tp'), may hold values from -2.9811459 to 2.9811459
- value_up: bfloat16 [128, 512], P(None, 'tp'), may hold values from -0.5 to 0.5
- rec_query: bfloat16 [2048, 256], P(None, 'tp'), may hold values from -0.125 to 0.125
- rec_key: bfloat16 [2048, 256], P(None, 'tp'), may hold values from -0.125 to 0.125
- rec_value: bfloat16 [2048, 512], P(None, 'tp'), may hold values from -0.125 to 0.125
- gate_weight: bfloat16 [2048, 4, 4], P(None, None, 'tp'), may hold values from -0.125 to 0.125
- forget_level: float32 [1024, 2, 4], P('sp', None, 'tp'), may hold values from 0 to 14
- head_gain: float32 [512], P('tp'), may hold values from 0.1 to 1.9
- init_state: float32 [2, 4, 64, 128], P(None, 'tp'), may hold values from -96 to 96
- init_norm: float32 [2, 4, 64], P(None, 'tp'), may hold values from -96 to 96
- out_attn: bfloat16 [512, 2048], P('tp'), may hold values from -0.25 to 0.25
- out_rec: bfloat16 [512, 2048], P('tp'), may hold values from -0.25 to 0.25
Outputs:
- mixed_out: bfloat16 [1024, 2048], P(('sp', 'tp'))
All inputs are finite; a program needn't handle non-finite values.
Results may differ from a plain program's by a relative error of at most 0.023.
Values may be sent and summed in bfloat16 or wider, within the bound.
A program may use at most 64 MiB of HBM per device.

v0:
```python
import math

import jax
import jax.numpy as jnp
from jax import lax
from jax.sharding import PartitionSpec as P

NOPE = 128
ROPE = 64
VH = 128
MK = 64
MV = 128
MBLOCK = 128


EPS = 1e-06
NEG = -1e30
HIGHEST = lax.Precision.HIGHEST


def prefix(x, axis, combine, identity, reverse):
    peers, mine = (lax.axis_size(axis), lax.axis_index(axis))
    everything = jax.tree.map(lambda part: lax.all_gather(part, axis), x)
    start = jax.tree.map(
        lambda part, zero: jnp.broadcast_to(jnp.asarray(zero, part.dtype), part.shape), x, identity
    )

    def lap(k, before):
        at = peers - 1 - k if reverse else k
        reached = at > mine if reverse else at < mine
        new = combine(before, jax.tree.map(lambda part: part[at], everything))
        return jax.tree.map(lambda a, b: jnp.where(reached, a, b), new, before)

    return lax.fori_loop(0, peers, lap, start)


def rms_rows(values, gains):
    return values * lax.rsqrt(jnp.mean(values * values, axis=-1, keepdims=True) + EPS) * gains


def rotate(values, positions):
    half_len = values.shape[-1] // 2
    frequency = 10000.0 ** (-jnp.arange(half_len, dtype=jnp.float32) / half_len)
    angles = positions.astype(jnp.float32)[:, None] * frequency[None, :]
    angles = jnp.concatenate([angles, angles], axis=-1)[:, None, :]
    turned = jnp.concatenate([-values[..., half_len:], values[..., :half_len]], axis=-1)
    return values * jnp.cos(angles) + turned * jnp.sin(angles)


def recurrence(query, keys_in, value_in, log_in, log_keep, c_start, n_start, m_start, floor_value):
    head_count, seq_len = log_in.shape
    block_count = seq_len // MBLOCK
    lower_mask = jnp.tril(jnp.ones((MBLOCK, MBLOCK), bool))

    def to_blocks(array):
        return jnp.moveaxis(
            array.reshape((head_count, block_count, MBLOCK) + array.shape[2:]), 1, 0
        )

    def one_step(carried, inputs):
        c_state, n_state, m_state = carried
        q_block, k_block, v_block, in_block, keep_block = inputs
        log_cum = jnp.cumsum(keep_block, axis=-1)
        log_decay = jnp.where(
            lower_mask, log_cum[:, :, None] - log_cum[:, None, :] + in_block[:, None, :], NEG
        )
        carry_log = log_cum + m_state[:, None]
        row_max = jnp.maximum(jnp.max(log_decay, axis=-1), carry_log)
        gated = jnp.einsum("htd,hsd->hts", q_block, k_block, precision=HIGHEST) * jnp.exp(
            log_decay - row_max[..., None]
        )
        carry_weight = jnp.exp(carry_log - row_max)
        numerator = jnp.einsum("hts,hse->hte", gated, v_block, precision=HIGHEST) + carry_weight[
            ..., None
        ] * jnp.einsum("htd,hde->hte", q_block, c_state, precision=HIGHEST)
        denominator = jnp.sum(gated, axis=-1) + carry_weight * jnp.einsum(
            "htd,hd->ht", q_block, n_state, precision=HIGHEST
        )
        result = (
            numerator
            / jnp.maximum(jnp.abs(denominator), floor_value * jnp.exp(-row_max))[..., None]
        )
        cum_end = log_cum[:, -1]
        weight_log = cum_end[:, None] - log_cum + in_block
        new_max = jnp.maximum(cum_end + m_state, jnp.max(weight_log, axis=-1))
        decay_all = jnp.exp(cum_end + m_state - new_max)
        in_weights = jnp.exp(weight_log - new_max[:, None])
        c_state = decay_all[:, None, None] * c_state + jnp.einsum(
            "hsd,hse->hde", k_block * in_weights[..., None], v_block, precision=HIGHEST
        )
        n_state = decay_all[:, None] * n_state + jnp.einsum(
            "hs,hsd->hd", in_weights, k_block, precision=HIGHEST
        )
        return ((c_state, n_state, new_max), result)

    inputs = tuple((to_blocks(array) for array in (query, keys_in, value_in, log_in, log_keep)))
    _, outputs = lax.scan(one_step, (c_start, n_start, m_start), inputs)
    return jnp.moveaxis(outputs, 0, 1).reshape(head_count, seq_len, -1)


def summary(keys_in, value_in, log_in, log_keep):
    log_cum = jnp.cumsum(log_keep, axis=-1)
    cum_end = log_cum[:, -1]
    weight_log = cum_end[:, None] - log_cum + log_in
    row_peak = jnp.max(weight_log, axis=-1)
    in_weights = jnp.exp(weight_log - row_peak[:, None])
    c_part = jnp.einsum(
        "hsd,hse->hde", keys_in * in_weights[..., None], value_in, precision=HIGHEST
    )
    n_part = jnp.einsum("hs,hsd->hd", in_weights, keys_in, precision=HIGHEST)
    return (c_part, n_part, row_peak, cum_end)


def combine(early_part, late_part):
    c_early, n_early, m_early, f_early = early_part
    c_late, n_late, m_late, f_late = late_part
    new_peak = jnp.maximum(f_late + m_early, m_late)
    carried = jnp.exp(f_late + m_early - new_peak)
    fresh = jnp.exp(m_late - new_peak)
    return (
        carried[:, None, None] * c_early + fresh[:, None, None] * c_late,
        carried[:, None] * n_early + fresh[:, None] * n_late,
        new_peak,
        f_early + f_late,
    )


def heads_first(product, head_width):
    rounded = lax.optimization_barrier(product.astype(jnp.bfloat16))
    return rounded.astype(jnp.float32).reshape(product.shape[0], -1, head_width).transpose(1, 0, 2)


def shards(
    rows_in,
    in_gain,
    query_down,
    query_gain,
    kv_down,
    kv_gain,
    rope_down,
    query_nope_up,
    query_rope_up,
    key_up,
    value_up,
    rec_query,
    rec_key,
    rec_value,
    gate_weight,
    forget_level,
    head_gain,
    init_state,
    init_norm,
    out_attn,
    out_rec,
):
    f32 = jnp.float32
    bf16 = jnp.bfloat16
    seq_rows = forget_level.shape[0]
    model_width = rows_in.shape[1]
    latent_kv = kv_down.shape[1]
    rope_width = rope_down.shape[1]
    attn_heads = value_up.shape[1] // VH
    rec_heads = head_gain.shape[0] // MV
    floor_value = float(seq_rows * lax.axis_size("sp")) ** 0.5
    normed = rms_rows(rows_in.astype(f32), in_gain).astype(bf16)
    gates_flat = gate_weight.reshape(model_width, 4 * rec_heads)
    projections = (query_down, kv_down, rope_down, rec_query, rec_key, rec_value, gates_flat)

    def project(row_piece):
        return jnp.concatenate(
            [jnp.dot(row_piece, weight, preferred_element_type=f32) for weight in projections],
            axis=1,
        )

    projected = project(lax.all_gather(normed, "tp", axis=0, tiled=True))
    splits = []
    offset = 0
    for weight in projections:
        splits.append(projected[:, offset : offset + weight.shape[1]])
        offset = offset + weight.shape[1]
    positions = lax.axis_index("sp") * seq_rows + jnp.arange(seq_rows, dtype=jnp.int32)
    q_latent = rms_rows(splits[0], query_gain).astype(bf16)
    kv_latent = rms_rows(splits[1], kv_gain).astype(bf16)
    key_rope = rotate(splits[2][:, None, :], positions)[:, 0, :].astype(bf16)
    query_nope = (
        jnp.dot(q_latent, query_nope_up, preferred_element_type=f32)
        .astype(bf16)
        .reshape(seq_rows, attn_heads, NOPE)
    )
    query_rope = rotate(
        jnp.dot(q_latent, query_rope_up, preferred_element_type=f32).reshape(
            seq_rows, attn_heads, ROPE
        ),
        positions,
    ).astype(bf16)
    query_abs = jnp.einsum(
        "thn,khn->thk",
        query_nope,
        key_up.reshape(latent_kv, attn_heads, NOPE),
        preferred_element_type=f32,
    ).astype(bf16)
    abs_rows = query_abs.reshape(seq_rows * attn_heads, latent_kv)
    rope_rows = query_rope.reshape(seq_rows * attn_heads, rope_width)
    score_scale = (NOPE + ROPE) ** (-0.5)
    query_count = seq_rows * attn_heads
    start_state = (
        jnp.full((query_count,), NEG, f32),
        jnp.zeros((query_count,), f32),
        jnp.zeros((query_count, latent_kv), f32),
    )
    contract = (((1,), (1,)), ((), ()))
    carried = start_state
    key_lat = lax.all_gather(kv_latent, "sp", axis=0, tiled=True)
    key_rot = lax.all_gather(key_rope, "sp", axis=0, tiled=True)
    total_rows = key_lat.shape[0]
    step_rows = math.gcd(total_rows, 2048)

    def one_block(running, key_block):
        row_peak, row_mass, row_accum = running
        lat_block, rot_block = key_block
        scores = lax.dot_general(abs_rows, lat_block, contract, preferred_element_type=f32)
        scores = (
            scores + lax.dot_general(rope_rows, rot_block, contract, preferred_element_type=f32)
        ) * score_scale
        new_peak = jnp.maximum(row_peak, jnp.max(scores, axis=1))
        expo_all = jnp.exp(scores - new_peak[:, None])
        shrink = jnp.exp(row_peak - new_peak)
        row_mass = row_mass * shrink + jnp.sum(expo_all, axis=1)
        row_accum = row_accum * shrink[:, None] + jnp.dot(
            expo_all.astype(bf16), lat_block, preferred_element_type=f32
        )
        return ((new_peak, row_mass, row_accum), None)

    key_blocks = (
        key_lat.reshape(total_rows // step_rows, step_rows, latent_kv),
        key_rot.reshape(total_rows // step_rows, step_rows, rope_width),
    )
    carried, _ = lax.scan(one_block, carried, key_blocks)
    row_peak, row_mass, row_accum = carried
    attended = (row_accum / row_mass[:, None]).astype(bf16).reshape(seq_rows, attn_heads, latent_kv)
    attention_out = (
        jnp.einsum(
            "thk,khv->thv",
            attended,
            value_up.reshape(latent_kv, attn_heads, VH),
            preferred_element_type=f32,
        )
        .astype(bf16)
        .reshape(seq_rows, attn_heads * VH)
    )
    rec_q = heads_first(splits[3], MK)
    rec_k = heads_first(splits[4], MK) * MK ** (-0.5)
    rec_v = heads_first(splits[5], MV)
    gate_pre = splits[6].reshape(seq_rows, 4, rec_heads)
    input_fwd = gate_pre[:, 0].T
    keep_fwd = jax.nn.log_sigmoid(gate_pre[:, 1] + forget_level[:, 0]).T
    input_bwd = gate_pre[:, 2].T[:, ::-1]
    keep_bwd = jax.nn.log_sigmoid(gate_pre[:, 3] + forget_level[:, 1]).T[:, ::-1]
    rev_q = rec_q[:, ::-1]
    rev_k = rec_k[:, ::-1]
    rev_v = rec_v[:, ::-1]
    identity = (
        jnp.zeros((rec_heads, MK, MV), f32),
        jnp.zeros((rec_heads, MK), f32),
        jnp.full((rec_heads,), NEG, f32),
        jnp.zeros((rec_heads,), f32),
    )
    own_fwd = summary(rec_k, rec_v, input_fwd, keep_fwd)
    own_bwd = summary(rev_k, rev_v, input_bwd, keep_bwd)
    prefix_state = prefix(own_fwd, "sp", combine, identity, False)
    suffix_state = prefix(own_bwd, "sp", combine, identity, True)
    zero_heads = jnp.zeros((rec_heads,), f32)
    start_fwd = combine((init_state[0], init_norm[0], zero_heads, zero_heads), prefix_state)
    start_bwd = combine((init_state[1], init_norm[1], zero_heads, zero_heads), suffix_state)
    forward_h = recurrence(
        rec_q,
        rec_k,
        rec_v,
        input_fwd,
        keep_fwd,
        start_fwd[0],
        start_fwd[1],
        start_fwd[2],
        floor_value,
    )
    backward_h = recurrence(
        rev_q,
        rev_k,
        rev_v,
        input_bwd,
        keep_bwd,
        start_bwd[0],
        start_bwd[1],
        start_bwd[2],
        floor_value,
    )[:, ::-1]
    summed = (forward_h + backward_h).transpose(1, 0, 2)
    recurrent_out = (
        rms_rows(summed, head_gain.reshape(rec_heads, MV))
        .astype(bf16)
        .reshape(seq_rows, rec_heads * MV)
    )
    mixed_out = lax.psum_scatter(
        (
            jnp.dot(attention_out, out_attn, preferred_element_type=f32)
            + jnp.dot(recurrent_out, out_rec, preferred_element_type=f32)
        ).astype(jnp.bfloat16),
        "tp",
        scatter_dimension=0,
        tiled=True,
    ).astype(jnp.float32)
    return mixed_out.astype(bf16)


def solution(mesh):
    in_specs = (
        P(("sp", "tp"), None),
        P(),
        P(),
        P(),
        P(),
        P(),
        P(),
        P(None, "tp"),
        P(None, "tp"),
        P(None, "tp"),
        P(None, "tp"),
        P(None, "tp"),
        P(None, "tp"),
        P(None, "tp"),
        P(None, None, "tp"),
        P("sp", None, "tp"),
        P("tp"),
        P(None, "tp", None, None),
        P(None, "tp", None),
        P("tp", None),
        P("tp", None),
    )
    out_specs = P(("sp", "tp"), None)
    return jax.shard_map(shards, mesh=mesh, in_specs=in_specs, out_specs=out_specs, check_vma=False)
```

profile of v0, /device:TPU:0, one launch (start us, length us, event | category | flops | bytes accessed | tf_op | source)
XLA Modules:
  0.0 260.4 jit_solution(8858869517683843515)
XLA Ops:
  6.6 1.1 fusion.28
  7.9 8.7 %all_gather.47 = bf16[128,2048]{1,0:T(8,128)(2,1)S(1)} all-gather(bf16[32,2048]{1,0:T(8,128)(2,1)S(1)} %fusion.30), channel_id=1, replica_groups=mesh['sp'=8,'tp'=4] {'tp'}, dimensions={0}, use_global_device_ids=true | all-gather | bytes 655360 | tf_op jit(solution)/shard_map/all_gather | solution.py:175
  18.2 1.4 fusion.94
  19.6 1.4 exponential_multiply_fusion
  21.3 1.5 convolution_bitcast_fusion.4
  25.3 1.4 bitcast_dynamic-update-slice_fusion.1
  26.7 1.2 bitcast_dynamic-update-slice_fusion
  27.9 1.2 fusion.121
  29.1 0.7 bitcast_multiply_fusion
  29.8 0.8 convolution_bitcast_fusion.2
  30.7 1.5 dynamic-update-slice.1
  32.1 1.4 dynamic-update-slice.4
  34.0 21.9 %all-reduce.6 = (f32[8]{0:T(128)S(1)}, f32[8]{0:T(128)S(1)}, f32[512]{0:T(512)S(1)}, f32[8]{0:T(128)S(1)}, f32[8]{0:T(128)S(1)}, /*index=5*/f32[512]{0:T(512)S(1)}) all-reduce(f32[8]{0:T(128)S(1)} %bitcast_dynamic-update-slice_fusion, f32[8]{0:T(128)S(1)} %dynamic-update-slice.4, ...), channel_id=1, replica_groups=mesh['sp'=8,'tp'=4] {'sp'}, use_global_device_ids=true, to_apply=%add.3 | all-reduce | flops 1056 | bytes 8448
  56.4 30.7 %all-gather.2 = f32[512,128]{1,0:T(8,128)S(1)} all-gather(f32[64,128]{1,0:T(8,128)S(1)} %fusion.52), channel_id=4, replica_groups=mesh['sp'=8,'tp'=4] {'sp'}, dimensions={0}, use_global_device_ids=true | all-gather | bytes 294912 | tf_op jit(solution)/shard_map/all_gather | solution.py:23
  87.2 26.6 %while.13 = (s32[]{:T(128)}, f32[1,64,128]{2,1,0:T(8,128)S(1)}, f32[1,64]{1,0:T(1,128)S(1)}, f32[1]{0:T(128)}, f32[1]{0:T(128)}, /*index=5*/s32[]{:T(128)}, f32[...) while((s32[]{:T(128)}, f32[1,64,128]{2,1,0:T(8,128)S(1)}, ...), condition=%wide.region_15.16_spmd.clone, body=%wide.region_14.15_spmd.clone.sunk | while | flops 41295 | bytes 99427 | solution.py:34
  107.2 0.7 constant_dynamic-slice_fusion.9
  114.1 30.9 %all-gather = f32[512,128]{1,0:T(8,128)S(1)} all-gather(f32[64,128]{1,0:T(8,128)S(1)} %fusion.57), channel_id=2, replica_groups=mesh['sp'=8,'tp'=4] {'sp'}, dimensions={0}, use_global_device_ids=true | all-gather | bytes 294912 | tf_op jit(solution)/shard_map/all_gather | solution.py:23
  145.0 24.9 %while.12 = (s32[]{:T(128)}, f32[1,64,128]{2,1,0:T(8,128)S(1)}, f32[1,64]{1,0:T(1,128)S(1)}, f32[1]{0:T(128)}, f32[1]{0:T(128)}, /*index=5*/s32[]{:T(128)}, f32[...) while((s32[]{:T(128)}, f32[1,64,128]{2,1,0:T(8,128)S(1)}, ...), condition=%wide.region_9.10_spmd.clone, body=%wide.region_8.9_spmd.clone.sunk | while | flops 41291 | bytes 99365 | solution.py:34
  173.2 26.2 %all_gather.49 = bf16[1024,64]{0,1:T(8,128)(2,1)S(1)} all-gather(bf16[128,64]{0,1:T(8,128)(2,1)S(1)} %fusion.44), channel_id=1, replica_groups=mesh['sp'=8,'tp'=4] {'sp'}, dimensions={0}, use_global_device_ids=true | all-gather | bytes 147456 | tf_op jit(solution)/shard_map/all_gather | solution.py:214
  200.1 26.4 %all_gather.48 = bf16[1024,128]{0,1:T(8,128)(2,1)S(1)} all-gather(bf16[128,128]{0,1:T(8,128)(2,1)S(1)} %multiply_convert_fusion.2), channel_id=1, replica_groups=mesh['sp'=8,'tp'=4] {'sp'}, dimensions={0}, use_global_device_ids=true | all-gather | bytes 294912 | tf_op jit(solution)/shard_map/all_gather | solution.py:213
  227.3 0.7 copy-done.19
  231.8 0.7 copy-done.1
  233.7 1.2 fusion.8
  234.9 18.7 %reduce-scatter.2.cloned.1.call-done = bf16[32,2048]{1,0:T(8,128)(2,1)} async-done(((bf16[128,2048]{1,0:T(8,128)(2,1)}), bf16[32,2048]{1,0:T(8,128)(2,1)}) %reduce-scatter.2.cloned.1.call-update) | async-done | bytes 131088 | tf_op jit(solution)/shard_map/reduce_scatter | solution.py:303
  (160 shorter events, 24.6 us)
Async XLA Ops:
  6.5 165.1 %copy-start = (bf16[2048,256]{1,0:T(8,128)(2,1)S(1)}, bf16[2048,256]{1,0:T(8,128)(2,1)}, u32[]{:S(2)}) copy-start(bf16[2048,256]{1,0:T(8,128)(2,1)} %param.27) | copy-start | bytes 3145732
  6.5 1.2 copy-start.4
  6.5 247.0 %reduce-scatter.2.cloned.1.call-start = ((), (), s32[]{:S(2)}) async-start(), calls=%async_computation.1 | async-start | bytes 655360 | tf_op jit(solution)/shard_map/reduce_scatter | solution.py:303
  6.6 1.2 copy-start.14
  7.9 8.7 %copy-start.13 = (bf16[2048,4,1]{0,1,2:T(4,128)(2,1)S(1)}, bf16[2048,4,1]{0,1,2:T(4,128)(2,1)}, u32[]{:S(2)}) copy-start(bf16[2048,4,1]{0,1,2:T(4,128)(2,1)} %param.39) | copy-start | bytes 49156
  16.5 0.7 copy-start.16
  16.5 4.4 %copy-start.6 = (bf16[2048,64]{0,1:T(8,128)(2,1)S(1)}, bf16[2048,64]{0,1:T(8,128)(2,1)}, u32[]{:S(2)}) copy-start(bf16[2048,64]{0,1:T(8,128)(2,1)} %param.37) | copy-start | bytes 786436
  16.8 39.1 %copy-start.2 = (bf16[2048,128]{1,0:T(8,128)(2,1)S(1)}, bf16[2048,128]{1,0:T(8,128)(2,1)}, u32[]{:S(2)}) copy-start(bf16[2048,128]{1,0:T(8,128)(2,1)} %param.38) | copy-start | bytes 1572868
  23.4 0.7 copy-start.21
  114.1 55.8 %copy-start.7 = (bf16[2048,64]{0,1:T(8,128)(2,1)S(1)}, bf16[2048,64]{0,1:T(8,128)(2,1)}, u32[]{:S(2)}) copy-start(bf16[2048,64]{0,1:T(8,128)(2,1)} %param.36) | copy-start | bytes 786436
  169.9 1.0 copy-start.8
  170.2 1.1 copy-start.3
  171.7 0.8 copy-start.11
  172.1 0.7 copy-start.15
  199.3 0.7 copy-start.17
  227.0 1.1 copy-start.20
  227.3 0.7 copy-start.19
  229.4 0.9 copy-start.9
  229.4 0.9 copy-start.12
  231.5 1.1 copy-start.1
  231.5 1.0 copy-start.10
  232.6 1.0 copy-start.5
  233.0 0.7 copy-start.18
Sparse Core Ops, SparseCore 0:
  235.0 18.5 reduce-scatter.1
where the time goes:
time: 262 us; the launch traced here: 260 us
  blocking collectives  145 us (55%)
  loops' own time  40.9 us (16%)
  local copies, waits for them, and re-layouts  23.7 us (9%)
  waiting for transfers between devices  18.7 us (7%)
  between operations  14.7 us (6%)
  matrix products  9.82 us (4%)
  other arithmetic  7.88 us (3%)
    all_gather x2, blocking collectives, prefix(): everything = jax.tree.map(lambda part: lax.all_gather(part, axis), x)  61.6 us
    another operation x2, loops' own time, prefix(): return lax.fori_loop(0, peers, lap, start)  40.9 us
    all_gather x1, blocking collectives, shards(): key_lat = lax.all_gather(kv_latent, 'sp', axis=0, tiled=True)  26.4 us
    all_gather x1, blocking collectives, shards(): key_rot = lax.all_gather(key_rope, 'sp', axis=0, tiled=True)  26.2 us
    unnamed x1, blocking collectives  21.9 us
    reduce_scatter x1, waiting for transfers between devices, shards(): lax.psum_scatter((jnp.dot(attention_out, out_attn, preferred_element_type...  18.7 us
    unnamed x57, local copies, waits for them, and re-layouts  11.7 us
    dynamic_slice x16, local copies, waits for them, and re-layouts, lap(): new = combine(before, jax.tree.map(lambda part: part[at], everything))  10.1 us
  transfers between devices with their start and end apart: 1, of which 1 were waited for; matrix products, arithmetic and copies ran while one was open for 0% of the time, Pallas kernels for 0%

commit v1 on v0

v1 whole, which is shorter than its diff:
```python
import functools

import jax
import jax.numpy as jnp
import numpy as np
from jax import lax
from jax.experimental import pallas as pl
from jax.experimental.pallas import tpu as pltpu
from jax.sharding import PartitionSpec as P

EPS = 1e-06
NEG = -1e30
HIGHEST = lax.Precision.HIGHEST
MESH = pl.DeviceIdType.MESH
F32 = jnp.float32
BF16 = jnp.bfloat16


def dot(a, b, **kw):
    return jnp.dot(a, b, preferred_element_type=F32, **kw)


def dot_t(a, b, **kw):
    return lax.dot_general(a, b, (((1,), (1,)), ((), ())), preferred_element_type=F32, **kw)


def dot_tn(a, b, **kw):
    return lax.dot_general(a, b, (((0,), (0,)), ((), ())), preferred_element_type=F32, **kw)


def rms(values, gains):
    return values * lax.rsqrt(jnp.mean(values * values, axis=-1, keepdims=True) + EPS) * gains


def turned(values):
    half = values.shape[-1] // 2
    return jnp.concatenate([-values[:, half:], values[:, :half]], axis=1)


def three_terms(value):
    high = value.astype(BF16).astype(F32)
    mid = (value - high).astype(BF16).astype(F32)
    return high, mid, value - high - mid


def kernel(n_sp, n_tp, names, *refs):
    count = len(names)
    hbm = dict(zip(names, refs[:count]))
    out_ref = refs[count]
    vm = dict(zip(names, refs[count + 1 : 2 * count + 1]))
    (
        xall,
        kvbuf,
        qcat,
        mix,
        smsg,
        sbuf,
        psend,
        pfull,
        prem,
        plast,
        plast_in,
        load_sem,
        x_send,
        x_recv,
        kv_send,
        kv_fwd,
        kv_recv,
        s_send,
        s_recv,
        p_send,
        p_recv,
        l_send,
        l_recv,
    ) = refs[2 * count + 1 :]
    half = n_tp // 2
    sp = lax.axis_index("sp")
    tp = lax.axis_index("tp")
    parity = lax.rem(tp, 2)
    partner_t = tp + 1 - 2 * parity
    partner = (sp, partner_t)
    rows = xall.shape[1]
    block = n_tp * rows
    plane = n_sp * half
    mine = sp * half + tp // 2

    loads = {
        name: pltpu.make_async_copy(hbm[name], vm[name], load_sem.at[i])
        for i, name in enumerate(names)
    }
    for name in names:
        loads[name].start()

    def peer_of(i):
        linear = lax.rem(mine + i, plane)
        return (linear // half, 2 * lax.rem(linear, half) + parity)

    barrier = pltpu.get_barrier_semaphore()

    def greet(i, c):
        pl.semaphore_signal(barrier, inc=1, device_id=peer_of(i), device_id_type=MESH)
        return c

    lax.fori_loop(1, plane, greet, 0)
    pl.semaphore_signal(barrier, inc=1, device_id=partner, device_id_type=MESH)

    def get(name):
        loads[name].wait()
        return vm[name]

    rows_in = get("rows_in")
    in_gain = get("in_gain")
    xall[tp] = rms(rows_in[...].astype(F32), in_gain[...]).astype(BF16)
    pl.semaphore_wait(barrier, plane)

    def remote(src, dst, send, recv, device):
        return pltpu.make_async_remote_copy(
            src_ref=src,
            dst_ref=dst,
            send_sem=send,
            recv_sem=recv,
            device_id=device,
            device_id_type=MESH,
        )

    def x_copy(slot, k, device):
        return remote(xall.at[slot], xall.at[slot], x_send.at[k], x_recv.at[slot], device)

    def tp_same(d):
        return lax.rem(tp + 2 * d, n_tp)

    x_out = []
    for d in range(1, half):
        x_out.append(x_copy(tp, d, (sp, tp_same(d))))
    x_out.append(x_copy(tp, 0, partner))
    for copy in x_out:
        copy.start()

    own = xall[tp]
    cos_l = get("cos_local")
    sin_l = get("sin_local")
    cos_b = get("cos_base")[sp]
    sin_b = get("sin_base")[sp]
    own_at = pl.ds(pl.multiple_of(tp * rows, rows), rows)
    kv = rms(dot(own, get("kv_down")[...]), get("kv_gain")[...])
    kr = dot(own, get("rope_down")[...])
    c_l = cos_l[own_at, :]
    s_l = sin_l[own_at, :]
    kr = kr * (cos_b * c_l - sin_b * s_l) + turned(kr) * (sin_b * c_l + cos_b * s_l)
    lat = kv.shape[1]
    rope = kr.shape[1]
    slot_me = sp * n_tp + tp
    kvbuf[slot_me, :, :lat] = kv.astype(BF16)
    kvbuf[slot_me, :, lat:] = jnp.concatenate([kr, jnp.zeros_like(kr)], axis=1).astype(BF16)

    def kv_copy(i):
        return remote(
            kvbuf.at[slot_me], kvbuf.at[slot_me], kv_send.at[i], kv_recv.at[slot_me], peer_of(i)
        )

    def slot_of(i):
        s, t = peer_of(i)
        return s * n_tp + t

    def kv_relay(i):
        slot = slot_of(i)
        return remote(kvbuf.at[slot], kvbuf.at[slot], kv_fwd.at[i], kv_recv.at[slot], partner)

    def start_kv(i, c):
        kv_copy(i).start()
        return c

    lax.fori_loop(1, plane, start_kv, 0)
    kv_relay(0).start()

    x_fwd = []
    for d in range(1, half):
        slot = tp_same(d)
        x_copy(slot, 0, partner).wait_recv()
        copy = x_copy(slot, half + d, partner)
        copy.start()
        x_fwd.append(copy)
    for d in range(half):
        x_copy(lax.rem(partner_t + 2 * d, n_tp), 0, partner).wait_recv()
    x = xall[...].reshape(block, xall.shape[2])

    gates = dot_t(get("gate_rows")[...], x)[:8]
    level = gates + get("levels")[...]
    keep = jnp.minimum(level, 0.0) - jnp.log1p(jnp.exp(-jnp.abs(level)))
    r_id = lax.broadcasted_iota(jnp.int32, (block, block), 0)
    c_id = lax.broadcasted_iota(jnp.int32, (block, block), 1)
    lower = r_id >= c_id
    upper = r_id <= c_id
    cum_f = dot(keep, upper.astype(F32), precision=HIGHEST)[1:2]
    cum_b = dot(keep, lower.astype(F32), precision=HIGHEST)[3:4]
    a_f = gates[0:1] - cum_f
    a_b = gates[2:3] - cum_b
    end_f = cum_f[:, block - 1 : block]
    end_b = cum_b[:, 0:1]
    peak_f = jnp.max(end_f + a_f, axis=1, keepdims=True)
    peak_b = jnp.max(end_b + a_b, axis=1, keepdims=True)
    e_f = jnp.exp(end_f + a_f - peak_f)
    e_b = jnp.exp(end_b + a_b - peak_b)
    row8 = lax.broadcasted_iota(jnp.int32, (8, block), 0)
    stack = jnp.where(
        row8 == 0,
        cum_f,
        jnp.where(row8 == 1, cum_b, jnp.where(row8 == 2, e_f, e_b)),
    )
    eye = (r_id == c_id).astype(F32)
    columns = dot_t(eye, stack, precision=HIGHEST)
    cum_f_col = columns[:, 0:1]
    cum_b_col = columns[:, 1:2]
    e_f_col = columns[:, 2:3]
    e_b_col = columns[:, 3:4]

    k = dot(x, get("rec_key")[...]).astype(BF16).astype(F32)
    k = k * k.shape[1] ** (-0.5)
    v = dot(x, get("rec_value")[...]).astype(BF16)
    k16 = k.astype(BF16)
    mk = k.shape[1]
    mv = v.shape[1]
    n_both = dot(stack.astype(BF16), k16)
    row16 = lax.broadcasted_iota(jnp.int32, (16, mv), 0)

    def put_state(d, e_col, n_row, peak, end):
        smsg[d, :mk, :] = dot_tn((k * e_col).astype(BF16), v).astype(BF16)
        p1, p2, p3 = three_terms(peak)
        f1, f2, f3 = three_terms(end)
        tail = jnp.concatenate([n_row, jnp.zeros((1, mv - mk), F32)], axis=1)
        tail = jnp.where(row16 == 0, tail, 0.0)
        for at, term in enumerate((p1, p2, p3, f1, f2, f3)):
            tail = jnp.where(row16 == at + 1, term, tail)
        smsg[d, mk:, :] = tail.astype(BF16)

    put_state(0, e_f_col, n_both[2:3], peak_f, end_f)
    put_state(1, e_b_col, n_both[3:4], peak_b, end_b)

    def s_copy(i):
        to = lax.rem(sp + i, n_sp)
        which = jnp.where(to > sp, 0, 1)
        return remote(smsg.at[which], sbuf.at[sp], s_send.at[i], s_recv.at[sp], (to, tp))

    def start_s(i, c):
        s_copy(i).start()
        return c

    lax.fori_loop(1, n_sp, start_s, 0)

    q_latent = rms(dot(x, get("query_down")[...]), get("query_gain")[...]).astype(BF16)
    q_nope = dot(q_latent, get("query_nope_up")[...]).astype(BF16)
    q_rope = dot(q_latent, get("query_rope_up")[...])
    cos_q = cos_b * cos_l[...] - sin_b * sin_l[...]
    sin_q = sin_b * cos_l[...] + cos_b * sin_l[...]
    q_rope = q_rope * cos_q + turned(q_rope) * sin_q
    qcat[:, :lat] = dot_t(q_nope, get("key_up")[...]).astype(BF16)
    qcat[:, lat:] = jnp.concatenate([q_rope, jnp.zeros_like(q_rope)], axis=1).astype(BF16)
    scale = (q_nope.shape[1] + rope) ** (-0.5)

    def relay(i, c):
        slot = slot_of(i)
        remote(
            kvbuf.at[slot], kvbuf.at[slot], kv_send.at[i], kv_recv.at[slot], partner
        ).wait_recv()
        kv_relay(i).start()
        return c

    lax.fori_loop(1, plane, relay, 0)

    q16 = dot(x, get("rec_query")[...]).astype(BF16)
    qf = q16.astype(F32)
    qk = dot_t(q16, k16)

    def within(mask, cum_col, a_row):
        decay = jnp.where(mask, cum_col + a_row, NEG)
        top = jnp.max(decay, axis=1, keepdims=True)
        gated = qk * jnp.exp(decay - top)
        return top, dot(gated.astype(BF16), v), jnp.sum(gated, axis=1, keepdims=True)

    in_f = within(lower, cum_f_col, a_f)
    in_b = within(upper, cum_b_col, a_b)

    def wait_kv(i, c):
        s = i // half
        t = 2 * lax.rem(i, half) + 1 - parity
        slot = s * n_tp + t
        remote(
            kvbuf.at[slot], kvbuf.at[slot], kv_fwd.at[0], kv_recv.at[slot], partner
        ).wait_recv()
        return c

    lax.fori_loop(0, plane, wait_kv, 0)
    queries = qcat[...]
    slots = n_sp * n_tp
    step = min(slots, 32)

    def attend(j, running):
        peak, mass, accum = running
        keys = kvbuf[pl.ds(j * step, step)].reshape(step * rows, kvbuf.shape[2])
        scores = dot_t(queries, keys) * scale
        new = jnp.maximum(peak, jnp.max(scores, axis=1, keepdims=True))
        expo = jnp.exp(scores - new)
        shrink = jnp.exp(peak - new)
        mass = mass * shrink + jnp.sum(expo, axis=1, keepdims=True)
        accum = accum * shrink + dot(expo.astype(BF16), keys[:, :lat])
        return new, mass, accum

    running = (
        jnp.full((block, 1), NEG, F32),
        jnp.zeros((block, 1), F32),
        jnp.zeros((block, lat), F32),
    )
    if slots == step:
        running = attend(0, running)
    else:
        running = lax.fori_loop(0, slots // step, attend, running)
    attended = (running[2] / running[1]).astype(BF16)
    vh = hbm["value_up"].shape[1]
    mix[:, :vh] = dot(attended, get("value_up")[...]).astype(BF16)

    def absorb(j, state):
        c_state, n_state, m_state = state
        remote(smsg.at[0], sbuf.at[j], s_send.at[0], s_recv.at[j], partner).wait_recv()
        c_new = sbuf[j, :mk, :].astype(F32)
        tail = sbuf[j, mk:, :].astype(F32)
        peak = tail[1:2, 0:1] + tail[2:3, 0:1] + tail[3:4, 0:1]
        end = tail[4:5, 0:1] + tail[5:6, 0:1] + tail[6:7, 0:1]
        top = jnp.maximum(end + m_state, peak)
        carried = jnp.exp(end + m_state - top)
        fresh = jnp.exp(peak - top)
        return (
            carried * c_state + fresh * c_new,
            carried * n_state + fresh * tail[0:1, :mk],
            top,
        )

    state0 = get("init_state")
    norm0 = get("init_norm")
    zero = jnp.zeros((1, 1), F32)
    fwd = lax.fori_loop(0, sp, absorb, (state0[0], norm0[0:1], zero))
    bwd = lax.fori_loop(
        0,
        n_sp - 1 - sp,
        lambda j, state: absorb(n_sp - 1 - j, state),
        (state0[1], norm0[1:2], zero),
    )
    floor = float(n_sp * block) ** 0.5

    def finish(inside, cum_col, state):
        top, num, den = inside
        c_state, n_state, m_state = state
        carry = cum_col + m_state
        new = jnp.maximum(top, carry)
        a = jnp.exp(top - new)
        b = jnp.exp(carry - new)
        num = a * num + b * dot(q16, c_state.astype(BF16))
        den = a * den + b * jnp.sum(qf * n_state, axis=1, keepdims=True)
        return num / jnp.maximum(jnp.abs(den), floor * jnp.exp(-new))

    total = finish(in_f, cum_f_col, fwd) + finish(in_b, cum_b_col, bwd)
    mix[:, vh:] = rms(total, get("head_gain")[...]).astype(BF16)

    w_attn = get("out_attn")
    w_rec = get("out_rec")
    pfull[...] = (dot(mix[:, :vh], w_attn[...]) + dot(mix[:, vh:], w_rec[...])).reshape(pfull.shape)
    p_out = []
    for d in range(half):
        to = lax.rem(partner_t + 2 * (d + 1), n_tp)
        psend[d] = pfull[to].astype(BF16)
        copy = remote(psend.at[d], prem.at[d], p_send.at[d], p_recv.at[d], partner)
        copy.start()
        p_out.append(copy)
    l_out = []
    for d in range(half):
        p_out[d].wait_recv()
        to = tp_same(d + 1)
        both = pfull[to] + prem[d].astype(F32)
        if d < half - 1:
            plast[d] = both.astype(BF16)
            copy = remote(plast.at[d], plast_in.at[d], l_send.at[d], l_recv.at[d], (sp, to))
            copy.start()
            l_out.append(copy)
    for copy in l_out:
        copy.wait_recv()
    for d in range(half - 1):
        both = both + plast_in[d].astype(F32)
    out_ref[...] = both.astype(BF16)

    for copy in x_out + x_fwd + p_out + l_out:
        copy.wait_send()

    def drain_kv(i, c):
        kv_copy(i).wait_send()
        return c

    def drain_relay(i, c):
        kv_relay(i).wait_send()
        return c

    def drain_s(i, c):
        s_copy(i).wait_send()
        return c

    lax.fori_loop(1, plane, drain_kv, 0)
    lax.fori_loop(0, plane, drain_relay, 0)
    lax.fori_loop(1, n_sp, drain_s, 0)


ORDER = (
    "rows_in",
    "in_gain",
    "kv_down",
    "kv_gain",
    "rope_down",
    "cos_local",
    "sin_local",
    "cos_base",
    "sin_base",
    "gate_rows",
    "levels",
    "rec_key",
    "rec_value",
    "query_down",
    "query_gain",
    "query_nope_up",
    "query_rope_up",
    "key_up",
    "rec_query",
    "value_up",
    "init_state",
    "init_norm",
    "head_gain",
    "out_attn",
    "out_rec",
)


def shards(
    n_sp,
    n_tp,
    rows_in,
    in_gain,
    query_down,
    query_gain,
    kv_down,
    kv_gain,
    rope_down,
    query_nope_up,
    query_rope_up,
    key_up,
    value_up,
    rec_query,
    rec_key,
    rec_value,
    gate_weight,
    forget_level,
    head_gain,
    init_state,
    init_norm,
    out_attn,
    out_rec,
):
    rows, width = rows_in.shape
    block = forget_level.shape[0]
    lat = kv_down.shape[1]
    rope = rope_down.shape[1]
    mk = rec_key.shape[1]
    mv = rec_value.shape[1]
    half = n_tp // 2
    pair = rope // 2
    frequency = 10000.0 ** (-np.arange(pair) / pair)
    frequency = np.concatenate([frequency, frequency])
    local = np.arange(block)[:, None] * frequency
    base = (np.arange(n_sp) * block)[:, None, None] * frequency
    gate_rows = jnp.pad(gate_weight[:, :, 0].T, ((0, 12), (0, 0)))
    levels = forget_level[:, :, 0].T
    levels = jnp.pad(levels[:, None, :], ((0, 0), (1, 0), (0, 0))).reshape(4, block)
    levels = jnp.pad(levels, ((0, 4), (0, 0)))
    arrays = dict(
        rows_in=rows_in,
        in_gain=in_gain[None],
        kv_down=kv_down,
        kv_gain=kv_gain[None],
        rope_down=rope_down,
        cos_local=jnp.asarray(np.cos(local), F32),
        sin_local=jnp.asarray(np.sin(local), F32),
        cos_base=jnp.asarray(np.cos(base), F32),
        sin_base=jnp.asarray(np.sin(base), F32),
        gate_rows=gate_rows,
        levels=levels,
        rec_key=rec_key,
        rec_value=rec_value,
        query_down=query_down,
        query_gain=query_gain[None],
        query_nope_up=query_nope_up,
        query_rope_up=query_rope_up,
        key_up=key_up,
        rec_query=rec_query,
        value_up=value_up,
        init_state=init_state[:, 0],
        init_norm=init_norm[:, 0],
        head_gain=head_gain[None],
        out_attn=out_attn,
        out_rec=out_rec,
    )
    operands = [arrays[name] for name in ORDER]
    plane = n_sp * half
    slots = n_sp * n_tp
    dma = pltpu.SemaphoreType.DMA
    scratch = [pltpu.VMEM(a.shape, a.dtype) for a in operands]
    scratch += [
        pltpu.VMEM((n_tp, rows, width), BF16),
        pltpu.VMEM((slots, rows, lat + 2 * rope), BF16),
        pltpu.VMEM((block, lat + 2 * rope), BF16),
        pltpu.VMEM((block, value_up.shape[1] + mv), BF16),
        pltpu.VMEM((2, mk + 16, mv), BF16),
        pltpu.VMEM((n_sp, mk + 16, mv), BF16),
        pltpu.VMEM((half, rows, width), BF16),
        pltpu.VMEM((n_tp, rows, width), F32),
        pltpu.VMEM((half, rows, width), BF16),
        pltpu.VMEM((half, rows, width), BF16),
        pltpu.VMEM((half, rows, width), BF16),
        dma((len(operands),)),
        dma((n_tp,)),
        dma((n_tp,)),
        dma((plane,)),
        dma((plane,)),
        dma((slots,)),
        dma((n_sp,)),
        dma((n_sp,)),
        dma((half,)),
        dma((half,)),
        dma((half,)),
        dma((half,)),
    ]
    return pl.pallas_call(
        functools.partial(kernel, n_sp, n_tp, ORDER),
        out_shape=jax.ShapeDtypeStruct((rows, width), BF16),
        in_specs=[pl.BlockSpec(memory_space=pl.ANY)] * len(operands),
        out_specs=pl.BlockSpec(memory_space=pltpu.VMEM),
        scratch_shapes=scratch,
        compiler_params=pltpu.CompilerParams(
            collective_id=0, has_side_effects=True, vmem_limit_bytes=60 * 2**20
        ),
    )(*operands)


def solution(mesh):
    in_specs = (
        P(("sp", "tp"), None),
        P(),
        P(),
        P(),
        P(),
        P(),
        P(),
        P(None, "tp"),
        P(None, "tp"),
        P(None, "tp"),
        P(None, "tp"),
        P(None, "tp"),
        P(None, "tp"),
        P(None, "tp"),
        P(None, None, "tp"),
        P("sp", None, "tp"),
        P("tp"),
        P(None, "tp", None, None),
        P(None, "tp", None),
        P("tp", None),
        P("tp", None),
    )
    return jax.shard_map(
        functools.partial(shards, mesh.shape["sp"], mesh.shape["tp"]),
        mesh=mesh,
        in_specs=in_specs,
        out_specs=P(("sp", "tp"), None),
        check_vma=False,
    )
```

time: 262 us -> 38.8 us (0.15)
  blocking collectives: 145 us -> 0 us
  loops' own time: 40.9 us -> 0 us
  Pallas kernels: 0 us -> 29.6 us
  waiting for transfers between devices: 18.7 us -> 0 us
  local copies, waits for them, and re-layouts: 23.7 us -> 9 us
  between operations: 14.7 us -> 0.02 us
  matrix products: 9.82 us -> 0 us
  other arithmetic: 7.88 us -> 0 us
    all_gather x5 -> x0, blocking collectives: 123 us -> none  [the longest x2 61.6 us: prefix(): everything = jax.tree.map(lambda part: lax.all_gather(part, axis), x)]
    another operation x2 -> x0, loops' own time: 40.9 us -> none  [prefix(): return lax.fori_loop(0, peers, lap, start)]
    pallas_call x0 -> x1, Pallas kernels: none -> 29.6 us  [shards(): pl.pallas_call(functools.partial(kernel, n_sp, n_tp, ORDER), out_shape=ja...]
    unnamed x1 -> x0, blocking collectives: 21.9 us -> none
    reduce_scatter x1 -> x0, waiting for transfers between devices: 18.7 us -> none  [shards(): lax.psum_scatter((jnp.dot(attention_out, out_attn, preferred_element_type...]
    dynamic_slice x16 -> x0, local copies, waits for them, and re-layouts: 10.1 us -> none  [lap(): new = combine(before, jax.tree.map(lambda part: part[at], everything))]
    dot_general x26 -> x0, matrix products: 9.82 us -> none  [the longest x2 2.33 us: summary(): n_part = jnp.einsum('hs,hsd->hd', in_weights, keys_in, precision=HIGHEST)]
    unnamed x57 -> x13, local copies, waits for them, and re-layouts: 11.7 us -> 7.75 us
  transfers between devices with their start and end apart: 1 -> 0, of which waited for: 1 -> 0; matrix products, arithmetic and copies ran while one was open for 0% -> 0% of each run, Pallas kernels for 0% -> 0%
where the time goes in v1:
time: 38.8 us; the launch traced here: 38.6 us
  Pallas kernels  29.6 us (76%)
  local copies, waits for them, and re-layouts  9 us (23%)
    pallas_call x1, Pallas kernels, shards(): pl.pallas_call(functools.partial(kernel, n_sp, n_tp, ORDER), out_shape=ja...  29.6 us
    unnamed x13, local copies, waits for them, and re-layouts  7.75 us

profile of v1, /device:TPU:0, one launch (start us, length us, event | category | flops | bytes accessed | tf_op | source)
XLA Modules:
  0.0 38.6 jit_solution(4370139650236566571)
XLA Ops:
  0.0 0.0 copy-start.3
  0.0 0.7 %copy-done.3 = f32[128,2,1]{0,2,1:T(1,128)S(1)} copy-done((f32[128,2,1]{0,2,1:T(1,128)S(1)}, f32[128,2,1]{0,2,1:T(1,128)}, u32[]{:S(2)}) %copy-start.3) | copy-done | bytes 1048
  0.7 0.6 %pad.14.refs_10_ = f32[8,128]{1,0:T(8,128)} pad(f32[4,128]{1,0:T(4,128)S(1)} %bitcast.20, f32[]{:T(128)} %constant.12.clone.1), padding=0_4x0_0 | pad | bytes 6148 | tf_op jit(solution)/shard_map/jit(_pad)/pad | solution.py:478
  1.3 0.0 copy-start.2
  1.3 1.5 %copy.29.refs_16_ = bf16[256,64]{1,0:T(8,128)(2,1)} copy(bf16[256,64]{0,1:T(8,128)(2,1)} %param.33) | data formatting | bytes 65536 | tf_op args[8]
  2.8 0.0 copy-done.2
  2.8 0.6 %pad.12.refs_9_ = bf16[16,2048]{1,0:T(8,128)(2,1)} pad(bf16[4,2048]{1,0:T(4,128)(2,1)S(1)} %bitcast.18, bf16[]{:T(256)} %constant.11.clone.1), padding=0_12x0_0 | pad | bytes 81922 | tf_op jit(solution)/shard_map/jit(_pad)/pad | solution.py:475
  3.4 0.0 copy-start
  3.4 2.0 %copy.27.refs_4_ = bf16[2048,64]{1,0:T(8,128)(2,1)} copy(bf16[2048,64]{0,1:T(8,128)(2,1)} %param.31) | data formatting | bytes 524288 | tf_op args[6]
  5.4 0.0 copy-done
  5.4 0.0 copy-start.1
  5.4 1.0 %copy.30.refs_18_ = bf16[2048,64]{1,0:T(8,128)(2,1)} copy(bf16[2048,64]{0,1:T(8,128)(2,1)S(1)} %copy-done) | data formatting | bytes 524288 | tf_op args[11]
  6.4 0.0 copy-done.1
  6.4 1.0 %copy.28.refs_11_ = bf16[2048,64]{1,0:T(8,128)(2,1)} copy(bf16[2048,64]{0,1:T(8,128)(2,1)S(1)} %copy-done.1) | data formatting | bytes 524288 | tf_op args[12]
  7.4 29.6 %shard_map.235 = bf16[32,2048]{1,0:T(8,128)(2,1)} custom-call(bf16[32,2048]{1,0:T(8,128)(2,1)} %refs_0_.1, f32[1,2048]{1,0:T(1,128)} %bitcast.19, bf16[2048,128]{1,0:T(8,128)(2,1)} %refs_2_.1, f32[1,128]{1,0:T(1,128)} %bitcast.24, bf16[2048,64]{1,0:T(8,128)(2,1)} %copy.27.refs_4_, f32[128,64]{1,0:T(8,128)} %constant.13.clone.refs_5_, ...), custom_call_target="tpu_custom_call" | custom-call | tf_op jit(solution)/shard_map/pallas_call | solution.py:536
  37.0 1.6 %copy.33 = bf16[32,2048]{1,0:T(8,128)(2,1)} copy(bf16[32,2048]{1,0:T(8,128)(2,1)} %shard_map.235) | data formatting | bytes 262144
  (1 shorter events, 0.0 us)
Async XLA Ops:
  0.0 0.7 %copy-start.3 = (f32[128,2,1]{0,2,1:T(1,128)S(1)}, f32[128,2,1]{0,2,1:T(1,128)}, u32[]{:S(2)}) copy-start(f32[128,2,1]{0,2,1:T(1,128)} %param.40) | copy-start | bytes 3076
  1.3 1.5 %copy-start.2 = (bf16[2048,4,1]{0,1,2:T(4,128)(2,1)S(1)}, bf16[2048,4,1]{0,1,2:T(4,128)(2,1)}, u32[]{:S(2)}) copy-start(bf16[2048,4,1]{0,1,2:T(4,128)(2,1)} %param.39) | copy-start | bytes 49156
  3.4 2.0 %copy-start = (bf16[2048,64]{0,1:T(8,128)(2,1)S(1)}, bf16[2048,64]{0,1:T(8,128)(2,1)}, u32[]{:S(2)}) copy-start(bf16[2048,64]{0,1:T(8,128)(2,1)} %param.36) | copy-start | bytes 786436
  5.4 1.0 %copy-start.1 = (bf16[2048,64]{0,1:T(8,128)(2,1)S(1)}, bf16[2048,64]{0,1:T(8,128)(2,1)}, u32[]{:S(2)}) copy-start(bf16[2048,64]{0,1:T(8,128)(2,1)} %param.37) | copy-start | bytes 786436

commit v2 on v1

--- a/solution.py
+++ b/solution.py
@@ -14,6 +14,7 @@
 MESH = pl.DeviceIdType.MESH
 F32 = jnp.float32
 BF16 = jnp.bfloat16
+STRIPS = 4
 
 
 def dot(a, b, **kw):
@@ -143,7 +144,7 @@
     sin_b = get("sin_base")[sp]
     own_at = pl.ds(pl.multiple_of(tp * rows, rows), rows)
     kv = rms(dot(own, get("kv_down")[...]), get("kv_gain")[...])
-    kr = dot(own, get("rope_down")[...])
+    kr = dot_t(own, get("rope_rows")[...])
     c_l = cos_l[own_at, :]
     s_l = sin_l[own_at, :]
     kr = kr * (cos_b * c_l - sin_b * s_l) + turned(kr) * (sin_b * c_l + cos_b * s_l)
@@ -184,8 +185,10 @@
         x_copy(lax.rem(partner_t + 2 * d, n_tp), 0, partner).wait_recv()
     x = xall[...].reshape(block, xall.shape[2])
 
-    gates = dot_t(get("gate_rows")[...], x)[:8]
-    level = gates + get("levels")[...]
+    gates = dot_t(get("gate_rows")[...], x)
+    levels = get("levels")
+    row4 = lax.broadcasted_iota(jnp.int32, gates.shape, 0)
+    level = gates + jnp.where(row4 < 2, levels[0], levels[1])
     keep = jnp.minimum(level, 0.0) - jnp.log1p(jnp.exp(-jnp.abs(level)))
     r_id = lax.broadcasted_iota(jnp.int32, (block, block), 0)
     c_id = lax.broadcasted_iota(jnp.int32, (block, block), 1)
@@ -214,7 +217,7 @@
     e_f_col = columns[:, 2:3]
     e_b_col = columns[:, 3:4]
 
-    k = dot(x, get("rec_key")[...]).astype(BF16).astype(F32)
+    k = dot_t(x, get("key_rows")[...]).astype(BF16).astype(F32)
     k = k * k.shape[1] ** (-0.5)
     v = dot(x, get("rec_value")[...]).astype(BF16)
     k16 = k.astype(BF16)
@@ -249,7 +252,7 @@
 
     q_latent = rms(dot(x, get("query_down")[...]), get("query_gain")[...]).astype(BF16)
     q_nope = dot(q_latent, get("query_nope_up")[...]).astype(BF16)
-    q_rope = dot(q_latent, get("query_rope_up")[...])
+    q_rope = dot_t(q_latent, get("query_rope_rows")[...])
     cos_q = cos_b * cos_l[...] - sin_b * sin_l[...]
     sin_q = sin_b * cos_l[...] + cos_b * sin_l[...]
     q_rope = q_rope * cos_q + turned(q_rope) * sin_q
@@ -267,7 +270,7 @@
 
     lax.fori_loop(1, plane, relay, 0)
 
-    q16 = dot(x, get("rec_query")[...]).astype(BF16)
+    q16 = dot_t(x, get("query_rows")[...]).astype(BF16)
     qf = q16.astype(F32)
     qk = dot_t(q16, k16)
 
@@ -317,6 +320,10 @@
     attended = (running[2] / running[1]).astype(BF16)
     vh = hbm["value_up"].shape[1]
     mix[:, :vh] = dot(attended, get("value_up")[...]).astype(BF16)
+
+    w_attn = get("out_attn")
+    w_rec = get("out_rec")
+    pfull[...] = dot(mix[:, :vh], w_attn[...]).reshape(pfull.shape)
 
     def absorb(j, state):
         c_state, n_state, m_state = state
@@ -360,31 +367,41 @@
     total = finish(in_f, cum_f_col, fwd) + finish(in_b, cum_b_col, bwd)
     mix[:, vh:] = rms(total, get("head_gain")[...]).astype(BF16)
 
-    w_attn = get("out_attn")
-    w_rec = get("out_rec")
-    pfull[...] = (dot(mix[:, :vh], w_attn[...]) + dot(mix[:, vh:], w_rec[...])).reshape(pfull.shape)
+    width = pfull.shape[2]
+    strip = width // STRIPS
     p_out = []
-    for d in range(half):
-        to = lax.rem(partner_t + 2 * (d + 1), n_tp)
-        psend[d] = pfull[to].astype(BF16)
-        copy = remote(psend.at[d], prem.at[d], p_send.at[d], p_recv.at[d], partner)
-        copy.start()
-        p_out.append(copy)
     l_out = []
-    for d in range(half):
-        p_out[d].wait_recv()
-        to = tp_same(d + 1)
-        both = pfull[to] + prem[d].astype(F32)
-        if d < half - 1:
-            plast[d] = both.astype(BF16)
-            copy = remote(plast.at[d], plast_in.at[d], l_send.at[d], l_recv.at[d], (sp, to))
+    for c in range(STRIPS):
+        cols = slice(c * strip, (c + 1) * strip)
+        add = dot(mix[:, vh:], w_rec[:, cols]).reshape(n_tp, rows, strip)
+        pfull[:, :, cols] = pfull[:, :, cols] + add
+        for d in range(half):
+            to = lax.rem(partner_t + 2 * (d + 1), n_tp)
+            psend[d, c] = pfull[to, :, cols].astype(BF16)
+            at = c * half + d
+            copy = remote(psend.at[d, c], prem.at[d, c], p_send.at[at], p_recv.at[at], partner)
+            copy.start()
+            p_out.append(copy)
+    for c in range(STRIPS):
+        cols = slice(c * strip, (c + 1) * strip)
+        for d in range(half - 1):
+            at = c * half + d
+            p_out[at].wait_recv()
+            to = tp_same(d + 1)
+            plast[d, c] = (pfull[to, :, cols] + prem[d, c].astype(F32)).astype(BF16)
+            copy = remote(
+                plast.at[d, c], plast_in.at[d, c], l_send.at[at], l_recv.at[at], (sp, to)
+            )
             copy.start()
             l_out.append(copy)
-    for copy in l_out:
-        copy.wait_recv()
-    for d in range(half - 1):
-        both = both + plast_in[d].astype(F32)
-    out_ref[...] = both.astype(BF16)
+    for c in range(STRIPS):
+        cols = slice(c * strip, (c + 1) * strip)
+        p_out[c * half + half - 1].wait_recv()
+        both = pfull[tp, :, cols] + prem[half - 1, c].astype(F32)
+        for d in range(half - 1):
+            l_out[c * (half - 1) + d].wait_recv()
+            both = both + plast_in[d, c].astype(F32)
+        out_ref[:, cols] = both.astype(BF16)
 
     for copy in x_out + x_fwd + p_out + l_out:
         copy.wait_send()
@@ -411,21 +428,21 @@
     "in_gain",
     "kv_down",
     "kv_gain",
-    "rope_down",
+    "rope_rows",
     "cos_local",
     "sin_local",
     "cos_base",
     "sin_base",
     "gate_rows",
     "levels",
-    "rec_key",
+    "key_rows",
     "rec_value",
     "query_down",
     "query_gain",
     "query_nope_up",
-    "query_rope_up",
+    "query_rope_rows",
     "key_up",
-    "rec_query",
+    "query_rows",
     "value_up",
     "init_state",
     "init_norm",
@@ -472,30 +489,26 @@
     frequency = np.concatenate([frequency, frequency])
     local = np.arange(block)[:, None] * frequency
     base = (np.arange(n_sp) * block)[:, None, None] * frequency
-    gate_rows = jnp.pad(gate_weight[:, :, 0].T, ((0, 12), (0, 0)))
-    levels = forget_level[:, :, 0].T
-    levels = jnp.pad(levels[:, None, :], ((0, 0), (1, 0), (0, 0))).reshape(4, block)
-    levels = jnp.pad(levels, ((0, 4), (0, 0)))
     arrays = dict(
         rows_in=rows_in,
         in_gain=in_gain[None],
         kv_down=kv_down,
         kv_gain=kv_gain[None],
-        rope_down=rope_down,
+        rope_rows=rope_down.T,
         cos_local=jnp.asarray(np.cos(local), F32),
         sin_local=jnp.asarray(np.sin(local), F32),
         cos_base=jnp.asarray(np.cos(base), F32),
         sin_base=jnp.asarray(np.sin(base), F32),
-        gate_rows=gate_rows,
-        levels=levels,
-        rec_key=rec_key,
+        gate_rows=gate_weight[:, :, 0].T,
+        levels=forget_level.transpose(1, 2, 0),
+        key_rows=rec_key.T,
         rec_value=rec_value,
         query_down=query_down,
         query_gain=query_gain[None],
         query_nope_up=query_nope_up,
-        query_rope_up=query_rope_up,
+        query_rope_rows=query_rope_up.T,
         key_up=key_up,
-        rec_query=rec_query,
+        query_rows=rec_query.T,
         value_up=value_up,
         init_state=init_state[:, 0],
         init_norm=init_norm[:, 0],
@@ -515,11 +528,11 @@
         pltpu.VMEM((block, value_up.shape[1] + mv), BF16),
         pltpu.VMEM((2, mk + 16, mv), BF16),
         pltpu.VMEM((n_sp, mk + 16, mv), BF16),
-        pltpu.VMEM((half, rows, width), BF16),
+        pltpu.VMEM((half, STRIPS, rows, width // STRIPS), BF16),
         pltpu.VMEM((n_tp, rows, width), F32),
-        pltpu.VMEM((half, rows, width), BF16),
-        pltpu.VMEM((half, rows, width), BF16),
-        pltpu.VMEM((half, rows, width), BF16),
+        pltpu.VMEM((half, STRIPS, rows, width // STRIPS), BF16),
+        pltpu.VMEM((half, STRIPS, rows, width // STRIPS), BF16),
+        pltpu.VMEM((half, STRIPS, rows, width // STRIPS), BF16),
         dma((len(operands),)),
         dma((n_tp,)),
         dma((n_tp,)),
@@ -528,10 +541,10 @@
         dma((slots,)),
         dma((n_sp,)),
         dma((n_sp,)),
-        dma((half,)),
-        dma((half,)),
-        dma((half,)),
-        dma((half,)),
+        dma((half * STRIPS,)),
+        dma((half * STRIPS,)),
+        dma((half * STRIPS,)),
+        dma((half * STRIPS,)),
     ]
     return pl.pallas_call(
         functools.partial(kernel, n_sp, n_tp, ORDER),

time: 38.8 us -> 31.6 us (0.81)
  local copies, waits for them, and re-layouts: 9 us -> 1.57 us
    unnamed x13 -> x1, local copies, waits for them, and re-layouts: 7.75 us -> 1.57 us
    pad x3 -> x0, local copies, waits for them, and re-layouts: 1.24 us -> none  [the longest x1 0.64 us: shards(): gate_rows = jnp.pad(gate_weight[:, :, 0].T, ((0, 12), (0, 0)))]
where the time goes in v2:
time: 31.6 us; the launch traced here: 31.4 us
  Pallas kernels  29.9 us (95%)
  local copies, waits for them, and re-layouts  1.57 us (5%)
    pallas_call x1, Pallas kernels, shards(): pl.pallas_call(functools.partial(kernel, n_sp, n_tp, ORDER), out_shape=ja...  29.9 us
    unnamed x1, local copies, waits for them, and re-layouts  1.57 us

profile of v2, /device:TPU:0, one launch (start us, length us, event | category | flops | bytes accessed | tf_op | source)
XLA Modules:
  0.0 31.4 jit_solution(8483578051810561561)
XLA Ops:
  0.0 29.9 %shard_map.235 = bf16[32,2048]{1,0:T(8,128)(2,1)} custom-call(bf16[32,2048]{1,0:T(8,128)(2,1)} %refs_0_.1, f32[1,2048]{1,0:T(1,128)} %bitcast.20, bf16[2048,128]{1,0:T(8,128)(2,1)} %refs_2_.1, f32[1,128]{1,0:T(1,128)} %bitcast.24, bf16[64,2048]{1,0:T(8,128)(2,1)} %bitcast.14, f32[128,64]{1,0:T(8,128)} %constant.8.clone.refs_5_, ...), custom_call_target="tpu_custom_call" | custom-call | tf_op jit(solution)/shard_map/pallas_call | solution.py:549
  29.9 1.6 %copy.27 = bf16[32,2048]{1,0:T(8,128)(2,1)} copy(bf16[32,2048]{1,0:T(8,128)(2,1)} %shard_map.235) | data formatting | bytes 262144

commit v3 on v2

--- a/solution.py
+++ b/solution.py
@@ -245,7 +245,7 @@
         return remote(smsg.at[which], sbuf.at[sp], s_send.at[i], s_recv.at[sp], (to, tp))
 
     def start_s(i, c):
-        s_copy(i).start()
+        s_copy(jnp.where(2 * sp < n_sp, n_sp - i, i)).start()
         return c
 
     lax.fori_loop(1, n_sp, start_s, 0)
@@ -326,31 +326,45 @@
     pfull[...] = dot(mix[:, :vh], w_attn[...]).reshape(pfull.shape)
 
     def absorb(j, state):
-        c_state, n_state, m_state = state
+        c_state, n_state, m_state, f_state = state
         remote(smsg.at[0], sbuf.at[j], s_send.at[0], s_recv.at[j], partner).wait_recv()
         c_new = sbuf[j, :mk, :].astype(F32)
         tail = sbuf[j, mk:, :].astype(F32)
-        peak = tail[1:2, 0:1] + tail[2:3, 0:1] + tail[3:4, 0:1]
+        peak = tail[1:2, 0:1] + tail[2:3, 0:1] + tail[3:4, 0:1] + f_state
         end = tail[4:5, 0:1] + tail[5:6, 0:1] + tail[6:7, 0:1]
-        top = jnp.maximum(end + m_state, peak)
-        carried = jnp.exp(end + m_state - top)
+        top = jnp.maximum(m_state, peak)
+        kept = jnp.exp(m_state - top)
         fresh = jnp.exp(peak - top)
         return (
-            carried * c_state + fresh * c_new,
-            carried * n_state + fresh * tail[0:1, :mk],
+            kept * c_state + fresh * c_new,
+            kept * n_state + fresh * tail[0:1, :mk],
+            top,
+            f_state + end,
+        )
+
+    def with_start(state, c_start, n_start):
+        c_state, n_state, m_state, f_state = state
+        top = jnp.maximum(m_state, f_state)
+        kept = jnp.exp(m_state - top)
+        carried = jnp.exp(f_state - top)
+        return (
+            kept * c_state + carried * c_start,
+            kept * n_state + carried * n_start,
             top,
         )
 
     state0 = get("init_state")
     norm0 = get("init_norm")
-    zero = jnp.zeros((1, 1), F32)
-    fwd = lax.fori_loop(0, sp, absorb, (state0[0], norm0[0:1], zero))
-    bwd = lax.fori_loop(
-        0,
-        n_sp - 1 - sp,
-        lambda j, state: absorb(n_sp - 1 - j, state),
-        (state0[1], norm0[1:2], zero),
+    empty = (
+        jnp.zeros((mk, mv), F32),
+        jnp.zeros((1, mk), F32),
+        jnp.full((1, 1), NEG, F32),
+        jnp.zeros((1, 1), F32),
     )
+    fwd = lax.fori_loop(0, sp, lambda i, state: absorb(sp - 1 - i, state), empty)
+    bwd = lax.fori_loop(sp + 1, n_sp, absorb, empty)
+    fwd = with_start(fwd, state0[0], norm0[0:1])
+    bwd = with_start(bwd, state0[1], norm0[1:2])
     floor = float(n_sp * block) ** 0.5
 
     def finish(inside, cum_col, state):
@@ -401,7 +415,7 @@
         for d in range(half - 1):
             l_out[c * (half - 1) + d].wait_recv()
             both = both + plast_in[d, c].astype(F32)
-        out_ref[:, cols] = both.astype(BF16)
+        out_ref[:, cols] = both
 
     for copy in x_out + x_fwd + p_out + l_out:
         copy.wait_send()
@@ -546,9 +560,9 @@
         dma((half * STRIPS,)),
         dma((half * STRIPS,)),
     ]
-    return pl.pallas_call(
+    total = pl.pallas_call(
         functools.partial(kernel, n_sp, n_tp, ORDER),
-        out_shape=jax.ShapeDtypeStruct((rows, width), BF16),
+        out_shape=jax.ShapeDtypeStruct((rows, width), F32),
         in_specs=[pl.BlockSpec(memory_space=pl.ANY)] * len(operands),
         out_specs=pl.BlockSpec(memory_space=pltpu.VMEM),
         scratch_shapes=scratch,
@@ -556,6 +570,7 @@
             collective_id=0, has_side_effects=True, vmem_limit_bytes=60 * 2**20
         ),
     )(*operands)
+    return total.astype(BF16)
 
 
 def solution(mesh):

time: 31.6 us -> 31.7 us (level)
  other arithmetic: 0 us -> 1.62 us
  local copies, waits for them, and re-layouts: 1.57 us -> 0 us
    convert_element_type x0 -> x1, other arithmetic: none -> 1.62 us  [shards(): return total.astype(BF16)]
    unnamed x1 -> x0, local copies, waits for them, and re-layouts: 1.57 us -> none
where the time goes in v3:
time: 31.7 us; the launch traced here: 31.5 us
  Pallas kernels  29.9 us (94%)
  other arithmetic  1.62 us (5%)
    pallas_call x1, Pallas kernels, shards(): pl.pallas_call(functools.partial(kernel, n_sp, n_tp, ORDER), out_shape=ja...  29.9 us
    convert_element_type x1, other arithmetic, shards(): return total.astype(BF16)  1.62 us

profile of v3, /device:TPU:0, one launch (start us, length us, event | category | flops | bytes accessed | tf_op | source)
XLA Modules:
  0.0 31.5 jit_solution(14891321739681813468)
XLA Ops:
  0.0 29.9 %shard_map.235 = f32[32,2048]{1,0:T(8,128)} custom-call(bf16[32,2048]{1,0:T(8,128)(2,1)} %refs_0_.1, f32[1,2048]{1,0:T(1,128)} %bitcast.20, bf16[2048,128]{1,0:T(8,128)(2,1)} %refs_2_.1, f32[1,128]{1,0:T(1,128)} %bitcast.24, bf16[64,2048]{1,0:T(8,128)(2,1)} %bitcast.14, f32[128,64]{1,0:T(8,128)} %constant.8.clone.refs_5_, f32[128,64]{1,0:T(8,128)} %constant.9.clone.refs_6_, ...), custom_call_target="tpu_custom_call" | custom-call | tf_op jit(solution)/shard_map/pallas_call | solution.py:563
  29.9 1.6 %convert_element_type.3 = bf16[32,2048]{1,0:T(8,128)(2,1)} convert(f32[32,2048]{1,0:T(8,128)} %shard_map.235) | non-fusion elementwise | flops 65536 | bytes 393216 | tf_op jit(solution)/shard_map/convert_element_type | solution.py:573
